TPU v7x, 32 devices: a whole 2x2x4 slice. The times are simulated.
32 devices in a mesh: ra: 4 (over z), cb: 8 (over y, x, core).
Axes of the slice: x: 2, y: 2, z: 4, core: 2. Of those that a mesh axis runs over, the one named last changes fastest.
Arguments:
- tokens: bfloat16 [2, 128, 3072], P(None, None, 'ra'), may hold values from -70 to 70
- norm_gain: float32 [2, 3072], P(None, 'ra'), may hold values from 0.1 to 1.9
- gate_weight: float32 [2, 3072, 8448], P(None, 'ra', 'cb'), may hold values from -0.109375 to 0.109375
- gate_scale: float32 [2, 8448], P(None, 'cb'), may hold values from 0.5 to 2
- up_weight: float32 [2, 3072, 8448], P(None, 'ra', 'cb'), may hold values from -0.109375 to 0.109375
- up_scale: float32 [2, 8448], P(None, 'cb'), may hold values from 0.5 to 2
- conv_weight: float32 [2, 3, 8448], P(None, None, 'cb'), may hold values from -3.5 to 3.5
- conv_bias: float32 [2, 8448], P(None, 'cb'), may hold values from -3 to 3
- down_weight: float32 [2, 8448, 3072], P(None, 'cb', 'ra'), may hold values from -0.0625 to 0.0625
- down_scale: float32 [2, 3072], P(None, 'ra'), may hold values from 0.5 to 2
Outputs:
- layer_output: bfloat16 [2, 128, 3072], P(None, None, 'ra')
All inputs are finite; a program needn't handle non-finite values.
Results may differ from a plain program's by a relative error of at most 0.014.
Values may be sent and summed in bfloat16 or wider, within the bound.
A program may use at most 64 MiB of HBM per device.

v0:
```python
import jax
import jax.numpy as jnp
from jax import lax
from jax.sharding import PartitionSpec as P

WIDTH = 3072


eps = 1e-06
residual_keep = 0.5


def causal_mix(gate_seq, conv_taps, conv_shift):
    count = conv_taps.shape[0]
    length = gate_seq.shape[1]
    padded = jnp.pad(gate_seq, ((0, 0), (count - 1, 0), (0, 0)))
    running = jnp.zeros_like(gate_seq) + conv_shift[None, None, :]
    for offset in range(count):
        running = (
            running + conv_taps[offset][None, None, :] * padded[:, offset : offset + length, :]
        )
    return running


def sublayer(current, norm_g, gate_w, gate_s, up_w, up_s, conv_taps, conv_shift, down_w, down_s):
    sequences, length, local_width = current.shape
    row_count = sequences * length
    values = current.astype(jnp.float32).reshape(row_count, local_width)
    squares = jnp.sum(values * values, axis=1)
    scaled = (values * norm_g[None, :]).astype(jnp.bfloat16)
    gate_part = jnp.dot(scaled, gate_w.astype(jnp.bfloat16), preferred_element_type=jnp.float32)
    up_part = jnp.dot(scaled, up_w.astype(jnp.bfloat16), preferred_element_type=jnp.float32)
    gate_sum, up_sum = (
        lax.psum_scatter(gate_part, "ra", scatter_dimension=1, tiled=True),
        lax.psum_scatter(up_part, "ra", scatter_dimension=1, tiled=True),
    )
    square_sum = lax.psum(squares, "ra")
    share_cols = gate_sum.shape[1]
    col_start = lax.axis_index("ra") * share_cols
    col_gate = lax.dynamic_slice_in_dim(gate_s, col_start, share_cols, 0)
    col_up = lax.dynamic_slice_in_dim(up_s, col_start, share_cols, 0)
    used_taps = lax.dynamic_slice_in_dim(conv_taps, col_start, share_cols, 1)
    used_shift = lax.dynamic_slice_in_dim(conv_shift, col_start, share_cols, 0)
    inverse_rms = lax.rsqrt(square_sum / WIDTH + eps)[:, None]
    gate_sum = gate_sum * inverse_rms * col_gate[None, :]
    up_sum = up_sum * inverse_rms * col_up[None, :]
    units = gate_sum.shape[1]
    conv_out = causal_mix(gate_sum.reshape(sequences, length, units), used_taps, used_shift)
    hidden_act = (jax.nn.silu(conv_out) * up_sum.reshape(sequences, length, units)).astype(
        jnp.bfloat16
    )
    hidden_act = hidden_act.reshape(row_count, units)
    hidden_act = lax.all_gather(hidden_act, "ra", axis=1, tiled=True)
    down_part = jnp.dot(hidden_act, down_w.astype(jnp.bfloat16), preferred_element_type=jnp.float32)
    down_sum = lax.psum(down_part, "cb")
    branch = down_sum * down_s[None, :]
    return (
        (residual_keep * values + branch)
        .astype(jnp.bfloat16)
        .reshape(sequences, length, local_width)
    )


def shards(
    tokens,
    norm_gain,
    gate_weight,
    gate_scale,
    up_weight,
    up_scale,
    conv_weight,
    conv_bias,
    down_weight,
    down_scale,
):
    current = tokens
    for layer_index in range(2):
        current = sublayer(
            current,
            norm_gain[layer_index],
            gate_weight[layer_index],
            gate_scale[layer_index],
            up_weight[layer_index],
            up_scale[layer_index],
            conv_weight[layer_index],
            conv_bias[layer_index],
            down_weight[layer_index],
            down_scale[layer_index],
        )
    return current


def solution(mesh):
    in_specs = (
        P(None, None, "ra"),
        P(None, "ra"),
        P(None, "ra", "cb"),
        P(None, "cb"),
        P(None, "ra", "cb"),
        P(None, "cb"),
        P(None, None, "cb"),
        P(None, "cb"),
        P(None, "cb", "ra"),
        P(None, "ra"),
    )
    out_specs = P(None, None, "ra")
    return jax.shard_map(shards, mesh=mesh, in_specs=in_specs, out_specs=out_specs, check_vma=False)
```

profile of v0, /device:TPU:0, one launch (start us, length us, event | category | flops | bytes accessed | tf_op | source)
XLA Modules:
  0.0 304.9 jit_solution(4028201805180705221)
XLA Ops:
  6.5 1.4 slice_reduce_fusion.1
  7.9 3.2 %convert.12 = bf16[2,768,1056]{1,2,0:T(8,128)(2,1)S(1)} convert(f32[2,768,1056]{1,2,0:T(8,128)} %param.12) | non-fusion elementwise | flops 1622016 | bytes 9732096 | tf_op jit(solution)/shard_map/convert.5
  11.1 1.2 convert_multiply_fusion.5
  12.4 0.7 copy-done
  13.1 1.6 fusion.5
  14.7 0.0 reduce-scatter.5.cloned.1.call-update
  14.7 0.0 reduce-scatter.7.cloned.1.call-start
  14.8 3.2 %convert.13 = bf16[2,768,1056]{1,2,0:T(8,128)(2,1)S(1)} convert(f32[2,768,1056]{1,2,0:T(8,128)} %param.14) | non-fusion elementwise | flops 1622016 | bytes 9732096 | tf_op jit(solution)/shard_map/convert.4
  17.9 1.7 copy-done.1
  19.6 1.6 fusion.4
  21.3 0.0 all-reduce.5.cloned.1.call-start
  21.4 3.4 %convert.14 = bf16[2,1056,768]{2,1,0:T(8,128)(2,1)S(1)} convert(f32[2,1056,768]{2,1,0:T(8,128)} %param.18) | non-fusion elementwise | flops 1622016 | bytes 9732096 | tf_op jit(solution)/shard_map/convert.3
  24.8 0.6 fusion.44
  25.4 0.6 fusion.45
  26.0 0.1 fusion.31
  26.1 0.1 fusion.29
  26.2 0.7 fusion.37
  26.9 13.9 %psum.28 = f32[256]{0:T(256)S(1)} all-reduce(f32[256]{0:T(256)S(1)} %bitcast.56), channel_id=1, replica_groups=mesh['ra'=4,'cb'=8] {'ra'}, use_global_device_ids=true, to_apply=%region_2.0 | all-reduce | flops 256 | bytes 2048 | tf_op jit(solution)/shard_map/psum | solution.py:37
  40.8 0.5 add_rsqrt_fusion.1
  41.4 4.3 %reduce-scatter.5.cloned.1.call-done = f32[256,264]{0,1:T(8,128)} async-done(((f32[256,1056]{0,1:T(8,128)}), f32[256,264]{0,1:T(8,128)}) %reduce-scatter.5.cloned.1.call-update) | async-done | bytes 270352 | tf_op jit(solution)/shard_map/reduce_scatter | solution.py:34
  45.7 28.7 %reduce-scatter.7.cloned.1.call-done = f32[256,264]{0,1:T(8,128)} async-done(((f32[256,1056]{0,1:T(8,128)}), f32[256,264]{0,1:T(8,128)}) %reduce-scatter.7.cloned.1.call-update) | async-done | bytes 270352 | tf_op jit(solution)/shard_map/reduce_scatter | solution.py:35
  74.3 1.9 multiply_multiply_fusion.3
  76.2 1.8 reshape.75
  78.0 0.8 reshape.76
  78.8 3.7 %fusion.28 = bf16[2,128,264]{1,0,2:T(2,128)(2,1)S(1)} fusion(f32[2,128,264]{1,0,2:T(2,128)} %reshape.76, f32[2,128,264]{1,0,2:T(2,128)} %reshape.75, f32[264]{0:T(512)} %get-tuple-element.10, f32[264]{0:T(512)S(1)} %get-tuple-element.9, f32[264]{0:T(512)S(1)} %get-tuple-element.8, f32[264]{0:T(512)S(1)} %get-tuple-element.32), kind=kLoop, calls=%fused_computation.49 | loop fusion | flops 811008 | bytes 680064 | tf_op jit(solution)/shard_map/convert_element_type | solution.py:49
  82.6 16.0 %all_gather.6 = bf16[256,1056]{0,1:T(8,128)(2,1)S(1)} all-gather(bf16[256,264]{0,1:T(8,128)(2,1)S(1)} %bitcast.54), channel_id=1, replica_groups=mesh['ra'=4,'cb'=8] {'ra'}, dimensions={1}, use_global_device_ids=true | all-gather | bytes 675840 | tf_op jit(solution)/shard_map/all_gather | solution.py:53
  98.6 1.6 fusion.3
  100.2 0.0 reduce-scatter.11.cloned.1.call-start
  100.3 54.1 %all-reduce.5.cloned.1.call-done = f32[256,768]{1,0:T(8,128)} async-done(((f32[256,768]{1,0:T(8,128)}), f32[256,768]{1,0:T(8,128)}) %all-reduce.5.cloned.1.call-update) | async-done | bytes 786448 | tf_op jit(solution)/shard_map/psum | solution.py:55
  154.4 1.6 fusion.11
  156.0 0.7 copy-done.2
  156.7 3.1 %fusion.1 = f32[256,1056]{0,1:T(8,128)} fusion(bf16[2,768,1056]{1,2,0:T(8,128)(2,1)} %copy-done.1, bf16[256,768]{1,0:T(8,128)(2,1)S(1)} %get-tuple-element.16, f32[768]{0:T(1024)S(1)} %copy-done.9), kind=kOutput, calls=%fused_computation.3 | convolution fusion | flops 415825920 | bytes 3099648 | tf_op jit(solution)/shard_map/dot_general | solution.py:32
  159.8 0.0 reduce-scatter.9.cloned.1.call-start
  159.9 3.2 %fusion.2 = f32[256,1056]{0,1:T(8,128)} fusion(bf16[2,768,1056]{1,2,0:T(8,128)(2,1)} %copy-done, bf16[256,768]{1,0:T(8,128)(2,1)} %copy-done.2, f32[768]{0:T(1024)S(1)} %copy-done.9), kind=kOutput, calls=%fused_computation.5 | convolution fusion | flops 415825920 | bytes 3099648 | tf_op jit(solution)/shard_map/dot_general | solution.py:31
  163.1 0.0 all-reduce.7.cloned.1.call-start
  163.1 1.4 fusion.35
  164.5 0.1 fusion.39
  164.6 12.2 %psum.30 = f32[256]{0:T(256)S(1)} all-reduce(f32[256]{0:T(256)S(1)} %get-tuple-element.15), channel_id=1, replica_groups=mesh['ra'=4,'cb'=8] {'ra'}, use_global_device_ids=true, to_apply=%region_7.8 | all-reduce | flops 256 | bytes 2048 | tf_op jit(solution)/shard_map/psum | solution.py:37
  176.8 10.4 %reduce-scatter.11.cloned.1.call-done = f32[256,264]{0,1:T(8,128)} async-done(((f32[256,1056]{0,1:T(8,128)}), f32[256,264]{0,1:T(8,128)}) %reduce-scatter.11.cloned.1.call-update) | async-done | bytes 270352 | tf_op jit(solution)/shard_map/reduce_scatter | solution.py:35
  187.2 28.5 %reduce-scatter.9.cloned.1.call-done = f32[256,264]{0,1:T(8,128)} async-done(((f32[256,1056]{0,1:T(8,128)}), f32[256,264]{0,1:T(8,128)}) %reduce-scatter.9.cloned.1.call-update) | async-done | bytes 270352 | tf_op jit(solution)/shard_map/reduce_scatter | solution.py:34
  215.8 1.9 multiply_multiply_fusion.1
  217.6 1.8 reshape.78
  219.4 0.8 reshape.79
  220.3 3.7 %fusion.27 = bf16[2,128,264]{1,0,2:T(2,128)(2,1)S(1)} fusion(f32[2,128,264]{1,0,2:T(2,128)} %reshape.79, f32[2,128,264]{1,0,2:T(2,128)} %reshape.78, f32[264]{0:T(512)S(1)} %get-tuple-element.7, f32[264]{0:T(512)S(1)} %get-tuple-element.6, f32[264]{0:T(512)S(1)} %get-tuple-element.5, f32[264]{0:T(512)S(1)} %get-tuple-element.33), kind=kLoop, calls=%fused_computation.48 | loop fusion | flops 811008 | bytes 680064 | tf_op jit(solution)/shard_map/convert_element_type | solution.py:49
  224.0 16.0 %all_gather.7 = bf16[256,1056]{0,1:T(8,128)(2,1)S(1)} all-gather(bf16[256,264]{0,1:T(8,128)(2,1)S(1)} %bitcast.55), channel_id=1, replica_groups=mesh['ra'=4,'cb'=8] {'ra'}, dimensions={1}, use_global_device_ids=true | all-gather | bytes 675840 | tf_op jit(solution)/shard_map/all_gather | solution.py:53
  240.0 1.6 fusion
  241.6 54.3 %all-reduce.7.cloned.1.call-done = f32[256,768]{1,0:T(8,128)} async-done(((f32[256,768]{1,0:T(8,128)}), f32[256,768]{1,0:T(8,128)}) %all-reduce.7.cloned.1.call-update) | async-done | bytes 786448 | tf_op jit(solution)/shard_map/psum | solution.py:55
  295.9 2.1 fusion.9
  (29 shorter events, 0.2 us)
Async XLA Ops:
  6.5 39.1 %reduce-scatter.5.cloned.1.call-start = ((), (), s32[]{:S(2)}) async-start(), calls=%async_computation.4 | async-start | bytes 1351680 | tf_op jit(solution)/shard_map/reduce_scatter | solution.py:34
  7.9 3.2 %copy-start.3 = (bf16[2,128,768]{2,1,0:T(8,128)(2,1)S(1)}, bf16[2,128,768]{2,1,0:T(8,128)(2,1)}, u32[]{:S(2)}) copy-start(bf16[2,128,768]{2,1,0:T(8,128)(2,1)} %param.10) | copy-start | bytes 1179652
  11.1 1.9 copy-start
  14.7 59.6 %reduce-scatter.7.cloned.1.call-start = ((), (), s32[]{:S(2)}) async-start(), calls=%async_computation.5 | async-start | bytes 1351680 | tf_op jit(solution)/shard_map/reduce_scatter | solution.py:35
  17.9 1.7 copy-start.1
  21.3 133.1 %all-reduce.5.cloned.1.call-start = ((), (), s32[]{:S(2)}) async-start(), calls=%async_computation.6 | async-start | bytes 1572864 | tf_op jit(solution)/shard_map/psum | solution.py:55
  21.4 3.4 %copy-start.5 = (f32[2,1056]{1,0:T(2,128)S(1)}, f32[2,1056]{1,0:T(2,128)}, u32[]{:S(2)}) copy-start(f32[2,1056]{1,0:T(2,128)} %param.13) | copy-start | bytes 25348
  21.4 4.0 %copy-start.6 = (f32[2,1056]{1,0:T(2,128)S(1)}, f32[2,1056]{1,0:T(2,128)}, u32[]{:S(2)}) copy-start(f32[2,1056]{1,0:T(2,128)} %param.15) | copy-start | bytes 25348
  21.4 4.7 %copy-start.7 = (f32[2,1056]{1,0:T(2,128)S(1)}, f32[2,1056]{1,0:T(2,128)}, u32[]{:S(2)}) copy-start(f32[2,1056]{1,0:T(2,128)} %param.17) | copy-start | bytes 25348
  21.4 4.8 %copy-start.4 = (f32[2,3,1056]{2,0,1:T(2,128)S(1)}, f32[2,3,1056]{2,0,1:T(2,128)}, u32[]{:S(2)}) copy-start(f32[2,3,1056]{2,0,1:T(2,128)} %param.16) | copy-start | bytes 76036
  98.6 1.7 copy-start.8
  100.2 56.5 %copy-start.9 = (f32[768]{0:T(1024)S(1)}, f32[768]{0:T(1024)}, u32[]{:S(2)}) copy-start(f32[768]{0:T(1024)} %get-tuple-element.13) | copy-start | bytes 9220
  100.2 87.0 %reduce-scatter.11.cloned.1.call-start = ((), (), s32[]{:S(2)}) async-start(), calls=%async_computation.8 | async-start | bytes 1351680 | tf_op jit(solution)/shard_map/reduce_scatter | solution.py:35
  156.0 0.7 copy-start.2
  159.8 56.0 %reduce-scatter.9.cloned.1.call-start = ((), (), s32[]{:S(2)}) async-start(), calls=%async_computation.7 | async-start | bytes 1351680 | tf_op jit(solution)/shard_map/reduce_scatter | solution.py:34
  163.1 132.8 %all-reduce.7.cloned.1.call-start = ((), (), s32[]{:S(2)}) async-start(), calls=%async_computation.9 | async-start | bytes 1572864 | tf_op jit(solution)/shard_map/psum | solution.py:55
Sparse Core Ops, SparseCore 0:
  14.8 30.7 reduce-scatter.4
  48.0 26.3 reduce-scatter.6
  100.4 53.9 all-reduce.4
  159.9 27.2 reduce-scatter.10
  189.4 26.3 reduce-scatter.8
  241.8 54.0 all-reduce.6
where the time goes:
time: 306 us; the launch traced here: 305 us
  waiting for transfers between devices  180 us (59%)
  blocking collectives  58.2 us (19%)
  other arithmetic  26.3 us (9%)
  between operations  13.7 us (4%)
  local copies, waits for them, and re-layouts  13.4 us (4%)
  matrix products  12.7 us (4%)
    psum x2, waiting for transfers between devices, sublayer(): down_sum = lax.psum(down_part, 'cb')  108 us
    reduce_scatter x2, waiting for transfers between devices, sublayer(): lax.psum_scatter(up_part, 'ra', scatter_dimension=1, tiled=True)  39.1 us
    reduce_scatter x2, waiting for transfers between devices, sublayer(): lax.psum_scatter(gate_part, 'ra', scatter_dimension=1, tiled=True)  32.8 us
    all_gather x2, blocking collectives, sublayer(): hidden_act = lax.all_gather(hidden_act, 'ra', axis=1, tiled=True)  32 us
    psum x2, blocking collectives, sublayer(): square_sum = lax.psum(squares, 'ra')  26.1 us
    another operation x3, other arithmetic  9.73 us
    convert_element_type x2, other arithmetic, sublayer(): (jax.nn.silu(conv_out) * up_sum.reshape(sequences, length, units)).astype...  7.42 us
  transfers between devices with their start and end apart: 6, of which 6 were waited for; matrix products, arithmetic and copies ran while one was open for 5% of the time, Pallas kernels for 0%

commit v1 on v0

--- a/solution.py
+++ b/solution.py
@@ -1,10 +1,11 @@
+import functools
+
 import jax
 import jax.numpy as jnp
 from jax import lax
+from jax.experimental import pallas as pl
+from jax.experimental.pallas import tpu as pltpu
 from jax.sharding import PartitionSpec as P
-
-WIDTH = 3072
-
 
 eps = 1e-06
 residual_keep = 0.5
@@ -41,7 +42,7 @@
     col_up = lax.dynamic_slice_in_dim(up_s, col_start, share_cols, 0)
     used_taps = lax.dynamic_slice_in_dim(conv_taps, col_start, share_cols, 1)
     used_shift = lax.dynamic_slice_in_dim(conv_shift, col_start, share_cols, 0)
-    inverse_rms = lax.rsqrt(square_sum / WIDTH + eps)[:, None]
+    inverse_rms = lax.rsqrt(square_sum / (local_width * lax.axis_size("ra")) + eps)[:, None]
     gate_sum = gate_sum * inverse_rms * col_gate[None, :]
     up_sum = up_sum * inverse_rms * col_up[None, :]
     units = gate_sum.shape[1]
@@ -90,6 +91,464 @@
     return current
 
 
+MESH = pl.DeviceIdType.MESH
+LANES = 128
+CHUNKS = 4
+LAG = dict(mix=1, act=2, down=3, fold=3, done=4)
+
+
+def fused(
+    chunks,
+    ra,
+    cb,
+    tokens,
+    norm_gain,
+    gate_weight,
+    gate_scale,
+    up_weight,
+    up_scale,
+    conv_weight,
+    conv_bias,
+    down_weight,
+    down_scale,
+    out,
+    stage_gate,
+    stage_up,
+    stage_down,
+    in_w,
+    out_w,
+    state,
+    own_part,
+    near_part,
+    far_send,
+    far_part,
+    hidden,
+    down_part,
+    down_recv,
+    conv_pad,
+    params,
+    load_sem,
+    near_s,
+    near_r,
+    far_s,
+    far_r,
+    hid_s,
+    hid_r,
+    red_s,
+    red_r,
+    out_s,
+    out_r,
+):
+    layers = 2
+    sequences, length, width = tokens.shape
+    units = gate_weight.shape[2]
+    main = units // LANES * LANES
+    rem = units - main
+    total_cols = 2 * main + LANES
+    step = length // chunks
+    rows = sequences * step
+    items = layers * chunks
+    share_rows, share_cols = down_recv.shape[2], down_recv.shape[3]
+    col_parts = width // share_cols
+    me = lax.axis_index("ra")
+    mine = lax.axis_index("cb")
+    inner = jnp.logical_and(me >= 1, me <= 2)
+    outer = jnp.logical_not(inner)
+    own_seq = me - 1
+
+    loads = []
+    for layer in range(layers):
+        for kind, (src, dst) in enumerate(
+            ((gate_weight, stage_gate), (up_weight, stage_up), (down_weight, stage_down))
+        ):
+            loads.append(
+                pltpu.make_async_copy(src.at[layer], dst.at[layer], load_sem.at[layer * 3 + kind])
+            )
+    for load in loads:
+        load.start()
+
+    barrier = pltpu.get_barrier_semaphore()
+    for d in range(1, ra):
+        pl.semaphore_signal(
+            barrier, inc=1, device_id={"ra": lax.rem(me + d, ra)}, device_id_type=MESH
+        )
+    for d in range(1, cb):
+        pl.semaphore_signal(
+            barrier, inc=1, device_id={"cb": lax.rem(mine + d, cb)}, device_id_type=MESH
+        )
+
+    for c in range(chunks):
+        for s in range(sequences):
+            state[c, s * step : (s + 1) * step, :] = tokens[s, c * step : (c + 1) * step, :]
+
+    def convert_in(layer):
+        loads[layer * 3].wait()
+        loads[layer * 3 + 1].wait()
+        block = 32
+
+        @pl.loop(0, width // block)
+        def _(i):
+            r = pl.ds(pl.multiple_of(i * block, block), block)
+            if main:
+                in_w[layer, r, 0:main] = stage_gate[layer, r, 0:main].astype(jnp.bfloat16)
+                in_w[layer, r, main : 2 * main] = stage_up[layer, r, 0:main].astype(jnp.bfloat16)
+            parts = [jnp.zeros((block, LANES - 2 * rem), jnp.float32)]
+            if rem:
+                parts = [
+                    stage_gate[layer, r, main:units],
+                    stage_up[layer, r, main:units],
+                ] + parts
+            in_w[layer, r, 2 * main :] = jnp.concatenate(parts, axis=1).astype(jnp.bfloat16)
+
+    def convert_out(layer):
+        loads[layer * 3 + 2].wait()
+        block = 32
+
+        @pl.loop(0, units // block)
+        def _(i):
+            r = pl.ds(pl.multiple_of(i * block, block), block)
+            out_w[layer, r, :] = stage_down[layer, r, :].astype(jnp.bfloat16)
+
+        pad = out_w.shape[1] - units
+        if pad:
+            out_w[layer, units:, :] = jnp.zeros((pad, width), jnp.bfloat16)
+
+    for layer in range(layers):
+        lines = [gate_scale[layer : layer + 1, :], up_scale[layer : layer + 1, :]]
+        lines.append(conv_bias[layer : layer + 1, :])
+        lines += [conv_weight[layer, j : j + 1, :] for j in range(conv_weight.shape[1])]
+        for row, line in enumerate(lines):
+            if rem:
+                zeros = jnp.zeros((1, LANES - rem), jnp.float32)
+                params[layer, row : row + 1, main:] = jnp.concatenate(
+                    [line[:, main:], zeros], axis=1
+                )
+            params[layer, row : row + 1, :main] = line[:, :main]
+
+    lane = lax.broadcasted_iota(jnp.int32, (1, LANES), 1)
+
+    def put_squares(tile, squares):
+        high = squares.astype(jnp.bfloat16).astype(jnp.float32)
+        low = squares - high
+        return jnp.where(lane == 2 * rem, high, jnp.where(lane == 2 * rem + 1, low, tile))
+
+    def get_squares(tile):
+        keep = jnp.logical_and(lane >= 2 * rem, lane < 2 * rem + 2)
+        return jnp.sum(jnp.where(keep, tile, 0.0), axis=1, keepdims=True)
+
+    def near_copy(k):
+        to = jnp.where(me == 0, 1, 2)
+        return pltpu.make_async_remote_copy(
+            src_ref=own_part.at[k],
+            dst_ref=near_part.at[k],
+            send_sem=near_s.at[k],
+            recv_sem=near_r.at[k],
+            device_id={"ra": to},
+            device_id_type=MESH,
+        )
+
+    def far_copy(k):
+        return pltpu.make_async_remote_copy(
+            src_ref=far_send.at[k],
+            dst_ref=far_part.at[k],
+            send_sem=far_s.at[k],
+            recv_sem=far_r.at[k],
+            device_id={"ra": 3 - me},
+            device_id_type=MESH,
+        )
+
+    def hid_rows(seq):
+        return pl.ds(pl.multiple_of(seq * step, step), step)
+
+    def hid_copy(k, d, seq):
+        return pltpu.make_async_remote_copy(
+            src_ref=hidden.at[k, hid_rows(seq)],
+            dst_ref=hidden.at[k, hid_rows(seq)],
+            send_sem=hid_s.at[k, d - 1],
+            recv_sem=hid_r.at[k, seq],
+            device_id={"ra": lax.rem(me + d, ra)},
+            device_id_type=MESH,
+        )
+
+    def share(p):
+        return (
+            pl.ds(pl.multiple_of(p // col_parts * share_rows, share_rows), share_rows),
+            pl.ds(pl.multiple_of(p % col_parts * share_cols, LANES), share_cols),
+        )
+
+    def red_copy(k, d):
+        to = lax.rem(mine + d, cb)
+        r, c = share(to)
+        return pltpu.make_async_remote_copy(
+            src_ref=down_part.at[k, r, c],
+            dst_ref=down_recv.at[k, d - 1],
+            send_sem=red_s.at[k, d - 1],
+            recv_sem=red_r.at[k, d - 1],
+            device_id={"cb": to},
+            device_id_type=MESH,
+        )
+
+    def out_copy(k, d, owner):
+        r, c = share(owner)
+        return pltpu.make_async_remote_copy(
+            src_ref=state.at[k + chunks, r, c],
+            dst_ref=state.at[k + chunks, r, c],
+            send_sem=out_s.at[k, d - 1],
+            recv_sem=out_r.at[k, d - 1],
+            device_id={"cb": lax.rem(mine + d, cb)},
+            device_id_type=MESH,
+        )
+
+    def enter(k):
+        layer = k // chunks
+        values = state[k].astype(jnp.float32)
+        squares = jnp.sum(values * values, axis=1, keepdims=True)
+        gain = norm_gain[pl.ds(layer, 1), :]
+        scaled = (values * gain).astype(jnp.bfloat16)
+        block = 512
+        for start in range(0, 2 * main, block):
+            stop = min(start + block, 2 * main)
+            own_part[k, :, start:stop] = jnp.dot(
+                scaled, in_w[layer, :, start:stop], preferred_element_type=jnp.float32
+            ).astype(jnp.bfloat16)
+        tile = jnp.dot(scaled, in_w[layer, :, 2 * main :], preferred_element_type=jnp.float32)
+        own_part[k, :, 2 * main :] = put_squares(tile, squares).astype(jnp.bfloat16)
+
+        @pl.when(outer)
+        def _():
+            near_copy(k).start()
+
+    def mix(k):
+        near_copy(k).wait_recv()
+        r = hid_rows(1 - own_seq)
+        both = own_part[k, r, : 2 * main].astype(jnp.float32) + near_part[
+            k, r, : 2 * main
+        ].astype(jnp.float32)
+        far_send[k, :, : 2 * main] = both.astype(jnp.bfloat16)
+        tile = own_part[k, r, 2 * main :].astype(jnp.float32) + near_part[k, r, 2 * main :].astype(
+            jnp.float32
+        )
+        far_send[k, :, 2 * main :] = put_squares(tile, get_squares(tile)).astype(jnp.bfloat16)
+        far_copy(k).start()
+
+    def act(k):
+        layer = k // chunks
+        far_copy(k).wait_recv()
+        r = hid_rows(own_seq)
+
+        def total(start, stop):
+            return (
+                own_part[k, r, start:stop].astype(jnp.float32)
+                + near_part[k, r, start:stop].astype(jnp.float32)
+                + far_part[k, :, start:stop].astype(jnp.float32)
+            )
+
+        tile = total(2 * main, total_cols)
+        inverse_rms = lax.rsqrt(get_squares(tile) / (width * ra) + eps)
+
+        @pl.when(k % chunks == 0)
+        def _():
+            conv_pad[0:8, :] = jnp.zeros((8, conv_pad.shape[1]), jnp.float32)
+
+        def piece(gate, up, start, stop):
+            def param(row):
+                return params[layer, row : row + 1, start:stop]
+
+            conv_pad[8 : 8 + step, start:stop] = gate * inverse_rms * param(0)
+            conv = param(2)
+            taps = conv_weight.shape[1]
+            for j in range(taps):
+                first = 8 - (taps - 1) + j
+                conv = conv + param(3 + j) * conv_pad[first : first + step, start:stop]
+            conv_pad[0:8, start:stop] = conv_pad[step : step + 8, start:stop]
+            value = conv / (1.0 + jnp.exp(-conv)) * (up * inverse_rms * param(1))
+            hidden[k, r, start:stop] = value.astype(jnp.bfloat16)
+
+        block = 256
+        for start in range(0, main, block):
+            stop = min(start + block, main)
+            piece(total(start, stop), total(main + start, main + stop), start, stop)
+        if rem:
+            piece(tile, pltpu.roll(tile, LANES - rem, axis=1), main, main + LANES)
+        for d in (2, 1, 3):
+            hid_copy(k, d, own_seq).start()
+
+    def down(k):
+        layer = k // chunks
+        for seq in range(sequences):
+
+            @pl.when(jnp.logical_not(jnp.logical_and(inner, own_seq == seq)))
+            def _():
+                hid_copy(k, 1, seq).wait_recv()
+
+        down_part[k] = jnp.dot(
+            hidden[k], out_w[layer], preferred_element_type=jnp.float32
+        ).astype(jnp.bfloat16)
+        for d in range(1, cb):
+            red_copy(k, d).start()
+
+    def fold(k):
+        layer = k // chunks
+        r, c = share(mine)
+        total = down_part[k, r, c].astype(jnp.float32)
+        for d in range(1, cb):
+            red_copy(k, d).wait_recv()
+            total = total + down_recv[k, d - 1].astype(jnp.float32)
+        kept = residual_keep * state[k, r, c].astype(jnp.float32)
+        state[k + chunks, r, c] = (kept + total * down_scale[pl.ds(layer, 1), c]).astype(
+            jnp.bfloat16
+        )
+        for d in range(1, cb):
+            out_copy(k, d, mine).start()
+
+    def done(k):
+        for d in range(1, cb):
+            out_copy(k, d, lax.rem(mine - d + cb, cb)).wait_recv()
+
+    convert_in(0)
+    pl.semaphore_wait(barrier, ra - 1 + cb - 1)
+
+    def at(slot, lag, work, extra=None):
+        item = slot - lag
+        good = jnp.logical_and(item >= 0, item < items)
+        if extra is not None:
+            good = jnp.logical_and(good, extra)
+
+        @pl.when(good)
+        def _():
+            work(item)
+
+    @pl.loop(0, items + LAG["done"])
+    def _(slot):
+        at(slot, LAG["done"], done)
+        at(slot, 0, enter)
+
+        @pl.when(slot == 0)
+        def _():
+            convert_out(0)
+
+        @pl.when(slot == 1)
+        def _():
+            convert_in(1)
+
+        @pl.when(slot == 2)
+        def _():
+            convert_out(1)
+
+        at(slot, LAG["down"], down)
+        at(slot, LAG["mix"], mix, inner)
+        at(slot, LAG["act"], act, inner)
+        at(slot, LAG["fold"], fold)
+
+    for c in range(chunks):
+        for s in range(sequences):
+            out[s, c * step : (c + 1) * step, :] = state[
+                items + c, s * step : (s + 1) * step, :
+            ]
+
+    @pl.loop(0, items)
+    def _(k):
+        @pl.when(outer)
+        def _():
+            near_copy(k).wait_send()
+
+        @pl.when(inner)
+        def _():
+            far_copy(k).wait_send()
+            for d in range(1, ra):
+                hid_copy(k, d, own_seq).wait_send()
+
+        for d in range(1, cb):
+            red_copy(k, d).wait_send()
+            out_copy(k, d, mine).wait_send()
+
+
+def share_shape(rows, width, parts):
+    for col_parts in range(1, parts + 1):
+        if parts % col_parts or width % (col_parts * LANES):
+            continue
+        if rows % (parts // col_parts * 16) == 0:
+            return rows * col_parts // parts, width // col_parts
+    return None
+
+
+def fused_shards(ra, cb, chunks, *operands):
+    tokens, gate_weight = operands[0], operands[2]
+    layers = 2
+    sequences, length, width = tokens.shape
+    units = gate_weight.shape[2]
+    main = units // LANES * LANES
+    total_cols = 2 * main + LANES
+    padded = main + (LANES if units > main else 0)
+    step = length // chunks
+    rows = sequences * step
+    items = layers * chunks
+    part = share_shape(rows, width, cb)
+    vmem = pl.BlockSpec(memory_space=pltpu.VMEM)
+    hbm = pl.BlockSpec(memory_space=pl.ANY)
+    dma = pltpu.SemaphoreType.DMA
+    bf16, f32 = jnp.bfloat16, jnp.float32
+    return pl.pallas_call(
+        functools.partial(fused, chunks, ra, cb),
+        out_shape=jax.ShapeDtypeStruct(tokens.shape, tokens.dtype),
+        in_specs=[vmem, vmem, hbm, vmem, hbm, vmem, vmem, vmem, hbm, vmem],
+        out_specs=vmem,
+        scratch_shapes=[
+            pltpu.VMEM((layers, width, units), f32),
+            pltpu.VMEM((layers, width, units), f32),
+            pltpu.VMEM((layers, units, width), f32),
+            pltpu.VMEM((layers, width, total_cols), bf16),
+            pltpu.VMEM((layers, padded, width), bf16),
+            pltpu.VMEM((items + chunks, rows, width), bf16),
+            pltpu.VMEM((items, rows, total_cols), bf16),
+            pltpu.VMEM((items, rows, total_cols), bf16),
+            pltpu.VMEM((items, step, total_cols), bf16),
+            pltpu.VMEM((items, step, total_cols), bf16),
+            pltpu.VMEM((items, rows, padded), bf16),
+            pltpu.VMEM((items, rows, width), bf16),
+            pltpu.VMEM((items, cb - 1) + part, bf16),
+            pltpu.VMEM((8 + step, padded), f32),
+            pltpu.VMEM((layers, 3 + operands[6].shape[1], padded), f32),
+            dma((layers * 3,)),
+            dma((items,)),
+            dma((items,)),
+            dma((items,)),
+            dma((items,)),
+            dma((items, ra - 1)),
+            dma((items, sequences)),
+            dma((items, cb - 1)),
+            dma((items, cb - 1)),
+            dma((items, cb - 1)),
+            dma((items, cb - 1)),
+        ],
+        compiler_params=pltpu.CompilerParams(
+            collective_id=0, has_side_effects=True, vmem_limit_bytes=60 * 1024 * 1024
+        ),
+    )(*operands)
+
+
+def fits(ra, cb, chunks, shape, local_width, local_units):
+    rem = local_units % LANES
+    return (
+        ra == 4
+        and shape[0] == 2
+        and shape[1] % (chunks * 16) == 0
+        and local_width % LANES == 0
+        and local_width % 32 == 0
+        and local_units % 32 == 0
+        and 2 * rem + 2 <= LANES
+        and local_units >= LANES
+        and share_shape(2 * shape[1] // chunks, local_width, cb) is not None
+    )
+
+
+def either(ra, cb, *operands):
+    tokens, gate_weight = operands[0], operands[2]
+    if fits(ra, cb, CHUNKS, tokens.shape, tokens.shape[2], gate_weight.shape[2]):
+        return fused_shards(ra, cb, CHUNKS, *operands)
+    return shards(*operands)
+
+
 def solution(mesh):
     in_specs = (
         P(None, None, "ra"),
@@ -104,4 +563,10 @@
         P(None, "ra"),
     )
     out_specs = P(None, None, "ra")
-    return jax.shard_map(shards, mesh=mesh, in_specs=in_specs, out_specs=out_specs, check_vma=False)
+    return jax.shard_map(
+        functools.partial(either, mesh.shape["ra"], mesh.shape["cb"]),
+        mesh=mesh,
+        in_specs=in_specs,
+        out_specs=out_specs,
+        check_vma=False,
+    )

time: 306 us -> 116 us (0.38)
  waiting for transfers between devices: 180 us -> 0 us
  Pallas kernels: 0 us -> 97 us
  blocking collectives: 58.2 us -> 0 us
  other arithmetic: 26.3 us -> 0 us
  between operations: 13.7 us -> 0.01 us
  matrix products: 12.7 us -> 0 us
  local copies, waits for them, and re-layouts: 13.4 us -> 18.3 us
    psum x2 -> x0, waiting for transfers between devices: 108 us -> none  [sublayer(): down_sum = lax.psum(down_part, 'cb')]
    pallas_call x0 -> x1, Pallas kernels: none -> 97 us  [fused_shards(): pl.pallas_call(functools.partial(fused, chunks, ra, cb), out_shape=jax.Sh...]
    reduce_scatter x4 -> x0, waiting for transfers between devices: 71.9 us -> none  [the longest x2 39.1 us: sublayer(): lax.psum_scatter(up_part, 'ra', scatter_dimension=1, tiled=True)]
    all_gather x2 -> x0, blocking collectives: 32 us -> none  [sublayer(): hidden_act = lax.all_gather(hidden_act, 'ra', axis=1, tiled=True)]
    psum x2 -> x0, blocking collectives: 26.1 us -> none  [sublayer(): square_sum = lax.psum(squares, 'ra')]
    unnamed x22 -> x4, local copies, waits for them, and re-layouts: 3.22 us -> 18.3 us
    dot_general x6 -> x0, matrix products: 12.7 us -> none  [the longest x2 4.82 us: sublayer(): jnp.dot(scaled, gate_w.astype(jnp.bfloat16), preferred_element_type=jnp.f...]
    another operation x3 -> x0, other arithmetic: 9.73 us -> none
  transfers between devices with their start and end apart: 6 -> 0, of which waited for: 6 -> 0; matrix products, arithmetic and copies ran while one was open for 5% -> 0% of each run, Pallas kernels for 0% -> 0%
where the time goes in v1:
time: 116 us; the launch traced here: 115 us
  Pallas kernels  97 us (84%)
  local copies, waits for them, and re-layouts  18.3 us (16%)
    pallas_call x1, Pallas kernels, fused_shards(): pl.pallas_call(functools.partial(fused, chunks, ra, cb), out_shape=jax.Sh...  97 us
    unnamed x4, local copies, waits for them, and re-layouts  18.3 us

profile of v1, /device:TPU:0, one launch (start us, length us, event | category | flops | bytes accessed | tf_op | source)
XLA Modules:
  0.0 115.3 jit_solution(17049062042013743186)
XLA Ops:
  0.0 1.4 %copy.13.conv_weight = f32[2,3,1056]{2,1,0:T(4,128)} copy(f32[2,3,1056]{2,0,1:T(2,128)} %param.16) | data formatting | bytes 50688 | tf_op args[6]
  1.4 7.6 %copy.11.gate_weight = f32[2,768,1056]{2,1,0:T(8,128)} copy(f32[2,768,1056]{1,2,0:T(8,128)} %param.12) | data formatting | bytes 12976128 | tf_op args[2]
  9.0 7.6 %copy.12.up_weight = f32[2,768,1056]{2,1,0:T(8,128)} copy(f32[2,768,1056]{1,2,0:T(8,128)} %param.14) | data formatting | bytes 12976128 | tf_op args[4]
  16.5 97.0 %shard_map.100 = bf16[2,128,768]{2,1,0:T(8,128)(2,1)} custom-call(bf16[2,128,768]{2,1,0:T(8,128)(2,1)} %tokens.1, f32[2,768]{1,0:T(2,128)} %norm_gain.1, f32[2,768,1056]{2,1,0:T(8,128)} %copy.11.gate_weight, f32[2,1056]{1,0:T(2,128)} %gate_scale.1, f32[2,768,1056]{2,1,0:T(8,128)} %copy.12.up_weight, f32[2,1056]{1,0:T(2,128)} %up_scale.1, ...), custom_call_target="tpu_custom_call" | custom-call | tf_op jit(solution)/shard_map/pallas_call | solution.py:491
  113.5 1.8 %copy.15 = bf16[2,128,768]{2,1,0:T(8,128)(2,1)} copy(bf16[2,128,768]{2,1,0:T(8,128)(2,1)} %shard_map.100) | data formatting | bytes 786432

commit v2 on v1

--- a/solution.py
+++ b/solution.py
@@ -93,8 +93,10 @@
 
 MESH = pl.DeviceIdType.MESH
 LANES = 128
-CHUNKS = 4
-LAG = dict(mix=1, act=2, down=3, fold=3, done=4)
+CHUNKS = 8
+LAG = dict(enter=0, mix=2, act=3, down=4, fold=6, done=8)
+ORDER = ("done", "mix", "enter", "act", "fold", "down")
+GAP = 8
 
 
 def fused(
@@ -179,7 +181,9 @@
 
     for c in range(chunks):
         for s in range(sequences):
-            state[c, s * step : (s + 1) * step, :] = tokens[s, c * step : (c + 1) * step, :]
+            state[c, s * step : (s + 1) * step, :] = tokens[
+                s, c * step : (c + 1) * step, :
+            ].astype(state.dtype)
 
     def convert_in(layer):
         loads[layer * 3].wait()
@@ -236,13 +240,15 @@
         keep = jnp.logical_and(lane >= 2 * rem, lane < 2 * rem + 2)
         return jnp.sum(jnp.where(keep, tile, 0.0), axis=1, keepdims=True)
 
-    def near_copy(k):
+    def near_copy(k, first):
         to = jnp.where(me == 0, 1, 2)
+        passed = jnp.where(me < 2, 1, 0)
+        r = hid_rows(passed if first else 1 - passed)
         return pltpu.make_async_remote_copy(
-            src_ref=own_part.at[k],
-            dst_ref=near_part.at[k],
-            send_sem=near_s.at[k],
-            recv_sem=near_r.at[k],
+            src_ref=own_part.at[k, r],
+            dst_ref=near_part.at[k, r],
+            send_sem=near_s.at[k, int(first)],
+            recv_sem=near_r.at[k, int(first)],
             device_id={"ra": to},
             device_id_type=MESH,
         )
@@ -316,10 +322,11 @@
 
         @pl.when(outer)
         def _():
-            near_copy(k).start()
+            near_copy(k, True).start()
+            near_copy(k, False).start()
 
     def mix(k):
-        near_copy(k).wait_recv()
+        near_copy(k, True).wait_recv()
         r = hid_rows(1 - own_seq)
         both = own_part[k, r, : 2 * main].astype(jnp.float32) + near_part[
             k, r, : 2 * main
@@ -333,6 +340,7 @@
 
     def act(k):
         layer = k // chunks
+        near_copy(k, False).wait_recv()
         far_copy(k).wait_recv()
         r = hid_rows(own_seq)
 
@@ -383,7 +391,7 @@
 
         down_part[k] = jnp.dot(
             hidden[k], out_w[layer], preferred_element_type=jnp.float32
-        ).astype(jnp.bfloat16)
+        ).astype(down_part.dtype)
         for d in range(1, cb):
             red_copy(k, d).start()
 
@@ -395,8 +403,10 @@
             red_copy(k, d).wait_recv()
             total = total + down_recv[k, d - 1].astype(jnp.float32)
         kept = residual_keep * state[k, r, c].astype(jnp.float32)
-        state[k + chunks, r, c] = (kept + total * down_scale[pl.ds(layer, 1), c]).astype(
-            jnp.bfloat16
+        state[k + chunks, r, c] = (
+            (kept + total * down_scale[pl.ds(layer, 1), c])
+            .astype(jnp.bfloat16)
+            .astype(state.dtype)
         )
         for d in range(1, cb):
             out_copy(k, d, mine).start()
@@ -408,49 +418,48 @@
     convert_in(0)
     pl.semaphore_wait(barrier, ra - 1 + cb - 1)
 
-    def at(slot, lag, work, extra=None):
-        item = slot - lag
-        good = jnp.logical_and(item >= 0, item < items)
-        if extra is not None:
-            good = jnp.logical_and(good, extra)
-
-        @pl.when(good)
-        def _():
-            work(item)
-
-    @pl.loop(0, items + LAG["done"])
+    works = dict(enter=enter, mix=mix, act=act, down=down, fold=fold, done=done)
+
+    @pl.loop(0, GAP + chunks + max(LAG.values()))
     def _(slot):
-        at(slot, LAG["done"], done)
-        at(slot, 0, enter)
-
-        @pl.when(slot == 0)
-        def _():
-            convert_out(0)
-
-        @pl.when(slot == 1)
-        def _():
-            convert_in(1)
-
-        @pl.when(slot == 2)
-        def _():
-            convert_out(1)
-
-        at(slot, LAG["down"], down)
-        at(slot, LAG["mix"], mix, inner)
-        at(slot, LAG["act"], act, inner)
-        at(slot, LAG["fold"], fold)
+        for name in ORDER:
+            place = slot - LAG[name]
+            late = place >= GAP
+            item = jnp.where(late, place - GAP + chunks, place)
+            good = jnp.logical_and(item >= 0, item < jnp.where(late, items, chunks))
+            if name in ("mix", "act"):
+                good = jnp.logical_and(good, inner)
+
+            @pl.when(good)
+            def _():
+                works[name](item)
+
+            if name == "enter":
+
+                @pl.when(slot == 0)
+                def _():
+                    convert_out(0)
+
+                @pl.when(slot == 1)
+                def _():
+                    convert_in(1)
+
+                @pl.when(slot == 2)
+                def _():
+                    convert_out(1)
 
     for c in range(chunks):
         for s in range(sequences):
             out[s, c * step : (c + 1) * step, :] = state[
                 items + c, s * step : (s + 1) * step, :
-            ]
+            ].astype(jnp.bfloat16)
 
     @pl.loop(0, items)
     def _(k):
         @pl.when(outer)
         def _():
-            near_copy(k).wait_send()
+            near_copy(k, True).wait_send()
+            near_copy(k, False).wait_send()
 
         @pl.when(inner)
         def _():
@@ -464,11 +473,12 @@
 
 
 def share_shape(rows, width, parts):
-    for col_parts in range(1, parts + 1):
-        if parts % col_parts or width % (col_parts * LANES):
-            continue
-        if rows % (parts // col_parts * 16) == 0:
-            return rows * col_parts // parts, width // col_parts
+    for tile, dtype in ((16, jnp.bfloat16), (8, jnp.float32)):
+        for col_parts in range(1, parts + 1):
+            if parts % col_parts or width % (col_parts * LANES):
+                continue
+            if rows % (parts // col_parts * tile) == 0:
+                return (rows * col_parts // parts, width // col_parts), dtype
     return None
 
 
@@ -483,7 +493,7 @@
     step = length // chunks
     rows = sequences * step
     items = layers * chunks
-    part = share_shape(rows, width, cb)
+    part, part_type = share_shape(rows, width, cb)
     vmem = pl.BlockSpec(memory_space=pltpu.VMEM)
     hbm = pl.BlockSpec(memory_space=pl.ANY)
     dma = pltpu.SemaphoreType.DMA
@@ -499,19 +509,19 @@
             pltpu.VMEM((layers, units, width), f32),
             pltpu.VMEM((layers, width, total_cols), bf16),
             pltpu.VMEM((layers, padded, width), bf16),
-            pltpu.VMEM((items + chunks, rows, width), bf16),
+            pltpu.VMEM((items + chunks, rows, width), part_type),
             pltpu.VMEM((items, rows, total_cols), bf16),
             pltpu.VMEM((items, rows, total_cols), bf16),
             pltpu.VMEM((items, step, total_cols), bf16),
             pltpu.VMEM((items, step, total_cols), bf16),
             pltpu.VMEM((items, rows, padded), bf16),
-            pltpu.VMEM((items, rows, width), bf16),
-            pltpu.VMEM((items, cb - 1) + part, bf16),
+            pltpu.VMEM((items, rows, width), part_type),
+            pltpu.VMEM((items, cb - 1) + part, part_type),
             pltpu.VMEM((8 + step, padded), f32),
             pltpu.VMEM((layers, 3 + operands[6].shape[1], padded), f32),
             dma((layers * 3,)),
-            dma((items,)),
-            dma((items,)),
+            dma((items, sequences)),
+            dma((items, sequences)),
             dma((items,)),
             dma((items,)),
             dma((items, ra - 1)),

time: 116 us -> 99.9 us (0.86)
  Pallas kernels: 97 us -> 81.3 us
    pallas_call x1, Pallas kernels: 97 us -> 81.3 us  [fused_shards(): pl.pallas_call(functools.partial(fused, chunks, ra, cb), out_shape=jax.Sh...]
where the time goes in v2:
time: 99.9 us; the launch traced here: 99.6 us
  Pallas kernels  81.3 us (81%)
  local copies, waits for them, and re-layouts  18.3 us (18%)
    pallas_call x1, Pallas kernels, fused_shards(): pl.pallas_call(functools.partial(fused, chunks, ra, cb), out_shape=jax.Sh...  81.3 us
    unnamed x4, local copies, waits for them, and re-layouts  18.3 us

profile of v2, /device:TPU:0, one launch (start us, length us, event | category | flops | bytes accessed | tf_op | source)
XLA Modules:
  0.0 99.6 jit_solution(18424858715793138024)
XLA Ops:
  0.0 1.4 %copy.13.conv_weight = f32[2,3,1056]{2,1,0:T(4,128)} copy(f32[2,3,1056]{2,0,1:T(2,128)} %param.16) | data formatting | bytes 50688 | tf_op args[6]
  1.4 7.6 %copy.11.gate_weight = f32[2,768,1056]{2,1,0:T(8,128)} copy(f32[2,768,1056]{1,2,0:T(8,128)} %param.12) | data formatting | bytes 12976128 | tf_op args[2]
  9.0 7.6 %copy.12.up_weight = f32[2,768,1056]{2,1,0:T(8,128)} copy(f32[2,768,1056]{1,2,0:T(8,128)} %param.14) | data formatting | bytes 12976128 | tf_op args[4]
  16.5 81.3 %shard_map.100 = bf16[2,128,768]{2,1,0:T(8,128)(2,1)} custom-call(bf16[2,128,768]{2,1,0:T(8,128)(2,1)} %tokens.1, f32[2,768]{1,0:T(2,128)} %norm_gain.1, f32[2,768,1056]{2,1,0:T(8,128)} %copy.11.gate_weight, f32[2,1056]{1,0:T(2,128)} %gate_scale.1, f32[2,768,1056]{2,1,0:T(8,128)} %copy.12.up_weight, f32[2,1056]{1,0:T(2,128)} %up_scale.1, ...), custom_call_target="tpu_custom_call" | custom-call | tf_op jit(solution)/shard_map/pallas_call | solution.py:501
  97.8 1.8 %copy.15 = bf16[2,128,768]{2,1,0:T(8,128)(2,1)} copy(bf16[2,128,768]{2,1,0:T(8,128)(2,1)} %shard_map.100) | data formatting | bytes 786432

commit v3 on v2

--- a/solution.py
+++ b/solution.py
@@ -143,7 +143,7 @@
 ):
     layers = 2
     sequences, length, width = tokens.shape
-    units = gate_weight.shape[2]
+    units = gate_weight.shape[1]
     main = units // LANES * LANES
     rem = units - main
     total_cols = 2 * main + LANES
@@ -190,19 +190,20 @@
         loads[layer * 3 + 1].wait()
         block = 32
 
-        @pl.loop(0, width // block)
+        @pl.loop(0, main // block)
         def _(i):
             r = pl.ds(pl.multiple_of(i * block, block), block)
-            if main:
-                in_w[layer, r, 0:main] = stage_gate[layer, r, 0:main].astype(jnp.bfloat16)
-                in_w[layer, r, main : 2 * main] = stage_up[layer, r, 0:main].astype(jnp.bfloat16)
-            parts = [jnp.zeros((block, LANES - 2 * rem), jnp.float32)]
-            if rem:
-                parts = [
-                    stage_gate[layer, r, main:units],
-                    stage_up[layer, r, main:units],
-                ] + parts
-            in_w[layer, r, 2 * main :] = jnp.concatenate(parts, axis=1).astype(jnp.bfloat16)
+            r2 = pl.ds(pl.multiple_of(main + i * block, block), block)
+            in_w[layer, r, :] = stage_gate[layer, r, :].astype(jnp.bfloat16)
+            in_w[layer, r2, :] = stage_up[layer, r, :].astype(jnp.bfloat16)
+
+        first = 2 * main
+        if rem:
+            in_w[layer, first : first + rem, :] = stage_gate[layer, main:, :].astype(jnp.bfloat16)
+            in_w[layer, first + rem : first + 2 * rem, :] = stage_up[layer, main:, :].astype(
+                jnp.bfloat16
+            )
+        in_w[layer, first + 2 * rem :, :] = jnp.zeros((LANES - 2 * rem, width), jnp.bfloat16)
 
     def convert_out(layer):
         loads[layer * 3 + 2].wait()
@@ -220,7 +221,7 @@
     for layer in range(layers):
         lines = [gate_scale[layer : layer + 1, :], up_scale[layer : layer + 1, :]]
         lines.append(conv_bias[layer : layer + 1, :])
-        lines += [conv_weight[layer, j : j + 1, :] for j in range(conv_weight.shape[1])]
+        lines += [conv_weight[j, layer : layer + 1, :] for j in range(conv_weight.shape[0])]
         for row, line in enumerate(lines):
             if rem:
                 zeros = jnp.zeros((1, LANES - rem), jnp.float32)
@@ -314,10 +315,18 @@
         block = 512
         for start in range(0, 2 * main, block):
             stop = min(start + block, 2 * main)
-            own_part[k, :, start:stop] = jnp.dot(
-                scaled, in_w[layer, :, start:stop], preferred_element_type=jnp.float32
+            own_part[k, :, start:stop] = lax.dot_general(
+                scaled,
+                in_w[layer, start:stop, :],
+                (((1,), (1,)), ((), ())),
+                preferred_element_type=jnp.float32,
             ).astype(jnp.bfloat16)
-        tile = jnp.dot(scaled, in_w[layer, :, 2 * main :], preferred_element_type=jnp.float32)
+        tile = lax.dot_general(
+            scaled,
+            in_w[layer, 2 * main :, :],
+            (((1,), (1,)), ((), ())),
+            preferred_element_type=jnp.float32,
+        )
         own_part[k, :, 2 * main :] = put_squares(tile, squares).astype(jnp.bfloat16)
 
         @pl.when(outer)
@@ -364,7 +373,7 @@
 
             conv_pad[8 : 8 + step, start:stop] = gate * inverse_rms * param(0)
             conv = param(2)
-            taps = conv_weight.shape[1]
+            taps = conv_weight.shape[0]
             for j in range(taps):
                 first = 8 - (taps - 1) + j
                 conv = conv + param(3 + j) * conv_pad[first : first + step, start:stop]
@@ -504,10 +513,10 @@
         in_specs=[vmem, vmem, hbm, vmem, hbm, vmem, vmem, vmem, hbm, vmem],
         out_specs=vmem,
         scratch_shapes=[
-            pltpu.VMEM((layers, width, units), f32),
-            pltpu.VMEM((layers, width, units), f32),
             pltpu.VMEM((layers, units, width), f32),
-            pltpu.VMEM((layers, width, total_cols), bf16),
+            pltpu.VMEM((layers, units, width), f32),
+            pltpu.VMEM((layers, units, width), f32),
+            pltpu.VMEM((layers, total_cols, width), bf16),
             pltpu.VMEM((layers, padded, width), bf16),
             pltpu.VMEM((items + chunks, rows, width), part_type),
             pltpu.VMEM((items, rows, total_cols), bf16),
@@ -534,7 +543,15 @@
         compiler_params=pltpu.CompilerParams(
             collective_id=0, has_side_effects=True, vmem_limit_bytes=60 * 1024 * 1024
         ),
-    )(*operands)
+    )(
+        *operands[:2],
+        jnp.swapaxes(gate_weight, 1, 2),
+        operands[3],
+        jnp.swapaxes(operands[4], 1, 2),
+        operands[5],
+        jnp.swapaxes(operands[6], 0, 1),
+        *operands[7:],
+    )
 
 
 def fits(ra, cb, chunks, shape, local_width, local_units):

time: 99.9 us -> 82.1 us (0.82)
  local copies, waits for them, and re-layouts: 18.3 us -> 1.77 us
  Pallas kernels: 81.3 us -> 80.2 us
    unnamed x4 -> x1, local copies, waits for them, and re-layouts: 18.3 us -> 1.77 us
    pallas_call x1, Pallas kernels: 81.3 us -> 80.2 us  [fused_shards(): pl.pallas_call(functools.partial(fused, chunks, ra, cb), out_shape=jax.Sh...]
where the time goes in v3:
time: 82.1 us; the launch traced here: 82 us
  Pallas kernels  80.2 us (98%)
  local copies, waits for them, and re-layouts  1.77 us (2%)
    pallas_call x1, Pallas kernels, fused_shards(): pl.pallas_call(functools.partial(fused, chunks, ra, cb), out_shape=jax.Sh...  80.2 us
    unnamed x1, local copies, waits for them, and re-layouts  1.77 us

profile of v3, /device:TPU:0, one launch (start us, length us, event | category | flops | bytes accessed | tf_op | source)
XLA Modules:
  0.0 82.0 jit_solution(13708562211739060017)
XLA Ops:
  0.0 80.2 %shard_map.100 = bf16[2,128,768]{2,1,0:T(8,128)(2,1)} custom-call(bf16[2,128,768]{2,1,0:T(8,128)(2,1)} %tokens.1, f32[2,768]{1,0:T(2,128)} %norm_gain.1, f32[2,1056,768]{2,1,0:T(8,128)} %bitcast.3, f32[2,1056]{1,0:T(2,128)} %gate_scale.1, f32[2,1056,768]{2,1,0:T(8,128)} %bitcast.4, f32[2,1056]{1,0:T(2,128)} %up_scale.1, f32[3,2,1056]{2,1,0:T(2,128)} %bitcast.5, ...), custom_call_target="tpu_custom_call" | custom-call | tf_op jit(solution)/shard_map/pallas_call | solution.py:510
  80.2 1.8 %copy.12 = bf16[2,128,768]{2,1,0:T(8,128)(2,1)} copy(bf16[2,128,768]{2,1,0:T(8,128)(2,1)} %shard_map.100) | data formatting | bytes 786432

commit v4 on v3

--- a/solution.py
+++ b/solution.py
@@ -103,17 +103,25 @@
     chunks,
     ra,
     cb,
+    far_tokens,
+    far_norm_gain,
+    gate_weight,
+    far_gate_scale,
+    up_weight,
+    far_up_scale,
+    far_conv_weight,
+    far_conv_bias,
+    down_weight,
+    far_down_scale,
+    out,
     tokens,
     norm_gain,
-    gate_weight,
     gate_scale,
-    up_weight,
     up_scale,
     conv_weight,
     conv_bias,
-    down_weight,
     down_scale,
-    out,
+    small_sem,
     stage_gate,
     stage_up,
     stage_down,
@@ -158,6 +166,32 @@
     outer = jnp.logical_not(inner)
     own_seq = me - 1
 
+    barrier = pltpu.get_barrier_semaphore()
+    for d in range(1, ra):
+        pl.semaphore_signal(
+            barrier, inc=1, device_id={"ra": lax.rem(me + d, ra)}, device_id_type=MESH
+        )
+    for d in range(1, cb):
+        pl.semaphore_signal(
+            barrier, inc=1, device_id={"cb": lax.rem(mine + d, cb)}, device_id_type=MESH
+        )
+
+    smalls = [
+        pltpu.make_async_copy(src, dst, small_sem.at[i])
+        for i, (src, dst) in enumerate(
+            (
+                (far_tokens, tokens),
+                (far_norm_gain, norm_gain),
+                (far_gate_scale, gate_scale),
+                (far_up_scale, up_scale),
+                (far_conv_weight, conv_weight),
+                (far_conv_bias, conv_bias),
+                (far_down_scale, down_scale),
+            )
+        )
+    ]
+    for small in smalls:
+        small.start()
     loads = []
     for layer in range(layers):
         for kind, (src, dst) in enumerate(
@@ -168,16 +202,8 @@
             )
     for load in loads:
         load.start()
-
-    barrier = pltpu.get_barrier_semaphore()
-    for d in range(1, ra):
-        pl.semaphore_signal(
-            barrier, inc=1, device_id={"ra": lax.rem(me + d, ra)}, device_id_type=MESH
-        )
-    for d in range(1, cb):
-        pl.semaphore_signal(
-            barrier, inc=1, device_id={"cb": lax.rem(mine + d, cb)}, device_id_type=MESH
-        )
+    for small in smalls:
+        small.wait()
 
     for c in range(chunks):
         for s in range(sequences):
@@ -507,12 +533,23 @@
     hbm = pl.BlockSpec(memory_space=pl.ANY)
     dma = pltpu.SemaphoreType.DMA
     bf16, f32 = jnp.bfloat16, jnp.float32
+    arranged = (
+        *operands[:2],
+        jnp.swapaxes(gate_weight, 1, 2),
+        operands[3],
+        jnp.swapaxes(operands[4], 1, 2),
+        operands[5],
+        jnp.swapaxes(operands[6], 0, 1),
+        *operands[7:],
+    )
     return pl.pallas_call(
         functools.partial(fused, chunks, ra, cb),
         out_shape=jax.ShapeDtypeStruct(tokens.shape, tokens.dtype),
-        in_specs=[vmem, vmem, hbm, vmem, hbm, vmem, vmem, vmem, hbm, vmem],
+        in_specs=[hbm] * 10,
         out_specs=vmem,
         scratch_shapes=[
+            *(pltpu.VMEM(arranged[i].shape, arranged[i].dtype) for i in (0, 1, 3, 5, 6, 7, 9)),
+            dma((7,)),
             pltpu.VMEM((layers, units, width), f32),
             pltpu.VMEM((layers, units, width), f32),
             pltpu.VMEM((layers, units, width), f32),
@@ -543,15 +580,7 @@
         compiler_params=pltpu.CompilerParams(
             collective_id=0, has_side_effects=True, vmem_limit_bytes=60 * 1024 * 1024
         ),
-    )(
-        *operands[:2],
-        jnp.swapaxes(gate_weight, 1, 2),
-        operands[3],
-        jnp.swapaxes(operands[4], 1, 2),
-        operands[5],
-        jnp.swapaxes(operands[6], 0, 1),
-        *operands[7:],
-    )
+    )(*arranged)
 
 
 def fits(ra, cb, chunks, shape, local_width, local_units):

time: 82.1 us -> 84 us (1.023)
  Pallas kernels: 80.2 us -> 82.1 us
    pallas_call x1, Pallas kernels: 80.2 us -> 82.1 us  [fused_shards(): pl.pallas_call(functools.partial(fused, chunks, ra, cb), out_shape=jax.Sh...]
where the time goes in v4:
time: 84 us; the launch traced here: 83.9 us
  Pallas kernels  82.1 us (98%)
  local copies, waits for them, and re-layouts  1.77 us (2%)
    pallas_call x1, Pallas kernels, fused_shards(): pl.pallas_call(functools.partial(fused, chunks, ra, cb), out_shape=jax.Sh...  82.1 us
    unnamed x1, local copies, waits for them, and re-layouts  1.77 us

profile of v4, /device:TPU:0, one launch (start us, length us, event | category | flops | bytes accessed | tf_op | source)
XLA Modules:
  0.0 83.9 jit_solution(6401279519320372528)
XLA Ops:
  0.0 82.1 %shard_map.100 = bf16[2,128,768]{2,1,0:T(8,128)(2,1)} custom-call(bf16[2,128,768]{2,1,0:T(8,128)(2,1)} %far_tokens.1, f32[2,768]{1,0:T(2,128)} %far_norm_gain.1, f32[2,1056,768]{2,1,0:T(8,128)} %bitcast.3, f32[2,1056]{1,0:T(2,128)} %far_gate_scale.1, f32[2,1056,768]{2,1,0:T(8,128)} %bitcast.4, f32[2,1056]{1,0:T(2,128)} %far_up_scale.1, ...), custom_call_target="tpu_custom_call" | custom-call | tf_op jit(solution)/shard_map/pallas_call | solution.py:545
  82.1 1.8 %copy.12 = bf16[2,128,768]{2,1,0:T(8,128)(2,1)} copy(bf16[2,128,768]{2,1,0:T(8,128)(2,1)} %shard_map.100) | data formatting | bytes 786432
